TPU v7x, 32 devices: a whole 2x2x4 slice. The times are simulated.
32 devices in a mesh: rep: 2 (over x), fs: 8 (over z, y), tp: 2 (over core).
Axes of the slice: x: 2, y: 2, z: 4, core: 2. Of those that a mesh axis runs over, the one named last changes fastest.
Arguments:
- tokens: bfloat16 [10240, 2048], P(('rep', 'fs', 'tp')), may hold values from -6 to 6
- mix_gain: float32 [2048], replicated, may hold values from 0.1 to 1.9
- w_bgate: bfloat16 [2048, 2048], P('fs', 'tp'), may hold values from -0.125 to 0.125
- w_cgate: bfloat16 [2048, 2048], P('fs', 'tp'), may hold values from -0.125 to 0.125
- w_value: bfloat16 [2048, 2048], P('fs', 'tp'), may hold values from -0.125 to 0.125
- conv_taps: float32 [3, 2048], replicated, may hold values from -3 to 3
- w_mixout: bfloat16 [2048, 2048], P('tp', 'fs'), may hold values from -0.125 to 0.125
- mlp_gain: float32 [2048], replicated, may hold values from 0.1 to 1.9
- w_gate: bfloat16 [2048, 2816], P('fs', 'tp'), may hold values from -0.125 to 0.125
- w_up: bfloat16 [2048, 2816], P('fs', 'tp'), may hold values from -0.125 to 0.125
- w_down: bfloat16 [2816, 2048], P('tp', 'fs'), may hold values from -0.109375 to 0.109375
Outputs:
- block_out: bfloat16 [10240, 2048], P(('rep', 'fs', 'tp'))
All inputs are finite; a program needn't handle non-finite values.
Results may differ from a plain program's by a relative error of at most 0.0085.
Values may be sent and summed in bfloat16 or wider, within the bound.
A program may use at most 128 MiB of HBM per device.

v0:
```python
import jax
import jax.numpy as jnp
from jax import lax
from jax.sharding import PartitionSpec as P


def rms_scale(matrix, gain):
    values = matrix.astype(jnp.float32)
    factor = lax.rsqrt(jnp.mean(values * values, axis=-1, keepdims=True) + 1e-06)
    return values * factor * gain


def causal_taps(mixed, filters):
    length = mixed.shape[-2]
    widths = [(0, 0)] * (mixed.ndim - 2) + [(2, 0), (0, 0)]
    padded = jnp.pad(mixed, widths)
    return (
        filters[0] * padded[..., 0:length, :]
        + filters[1] * padded[..., 1 : length + 1, :]
        + filters[2] * padded[..., 2 : length + 2, :]
    )


def gather_rows(normed):
    return lax.all_gather(normed, "tp", axis=0, tiled=True)


def project_in(gathered, stacked):
    return jnp.einsum(
        "td,kdc->ktc",
        gathered,
        lax.all_gather(stacked, "fs", axis=1, tiled=True),
        preferred_element_type=jnp.float32,
    )


def collect_out(weight):
    return lax.all_gather(weight, "fs", axis=1, tiled=True)


def sum_parts(local_cols, weight):
    return lax.psum_scatter(
        jnp.dot(local_cols, weight, preferred_element_type=jnp.float32).astype(jnp.bfloat16),
        "tp",
        scatter_dimension=0,
        tiled=True,
    ).astype(jnp.float32)


def on_device(
    tokens, mix_gain, w_bgate, w_cgate, w_value, conv_taps, w_mixout, mlp_gain, w_gate, w_up, w_down
):
    normed = rms_scale(tokens, mix_gain).astype(jnp.bfloat16)
    gathered = gather_rows(normed)
    projected = project_in(gathered, jnp.stack([w_bgate, w_cgate, w_value])).astype(jnp.bfloat16)
    channels = projected.shape[2]
    channel_taps = lax.dynamic_slice_in_dim(conv_taps, lax.axis_index("tp") * channels, channels, 1)
    mixed_in = projected[1].astype(jnp.float32) * projected[2].astype(jnp.float32)
    gated = (projected[0].astype(jnp.float32) * causal_taps(mixed_in, channel_taps)).astype(
        jnp.bfloat16
    )
    residual = tokens.astype(jnp.float32) + sum_parts(gated, collect_out(w_mixout))
    normed_two = rms_scale(residual, mlp_gain).astype(jnp.bfloat16)
    gathered_two = gather_rows(normed_two)
    gate_up = project_in(gathered_two, jnp.stack([w_gate, w_up]))
    hidden = (jax.nn.silu(gate_up[0]) * gate_up[1]).astype(jnp.bfloat16)
    result = residual + 0.5 * sum_parts(hidden, collect_out(w_down))
    return result.astype(jnp.bfloat16)


def solution(mesh):
    return jax.shard_map(
        on_device,
        mesh=mesh,
        in_specs=(
            P(("rep", "fs", "tp"), None),
            P(),
            P("fs", "tp"),
            P("fs", "tp"),
            P("fs", "tp"),
            P(),
            P("tp", "fs"),
            P(),
            P("fs", "tp"),
            P("fs", "tp"),
            P("tp", "fs"),
        ),
        out_specs=P(("rep", "fs", "tp"), None),
        check_vma=False,
    )
```

profile of v0, /device:TPU:0, one launch (start us, length us, event | category | flops | bytes accessed | tf_op | source)
XLA Modules:
  0.0 599.1 jit_solution(9736600943579483417)
XLA Ops:
  6.5 1.8 fusion.2
  8.3 2.7 fusion.4
  11.1 0.0 all-gather.7.cloned.1.call-start
  11.2 1.3 pad_maximum_fusion
  12.5 0.0 all-gather.11.cloned.1.call-start
  12.6 0.7 all-gather.11.cloned.1.call-update
  13.3 0.9 constant_dynamic-slice_fusion
  14.2 11.1 %all-gather.9.cloned.1.call-done = bf16[640,2048]{1,0:T(8,128)(2,1)} async-done(((bf16[320,2048]{1,0:T(8,128)(2,1)}), bf16[640,2048]{1,0:T(8,128)(2,1)}) %all-gather.9.cloned.1.call-update) | async-done | bytes 2621456 | tf_op jit(solution)/shard_map/all_gather | solution.py:25
  25.3 179.5 %all-gather.7.cloned.1.call-done = bf16[3,2048,1024]{2,1,0:T(8,128)(2,1)} async-done(((bf16[3,256,1024]{2,1,0:T(8,128)(2,1)}), bf16[3,2048,1024]{2,1,0:T(8,128)(2,1)}) %all-gather.7.cloned.1.call-update) | async-done | bytes 12582928 | tf_op jit(solution)/shard_map/all_gather | solution.py:32
  204.8 12.0 %convert_bitcast_fusion = bf16[3,640,1024]{2,1,0:T(8,128)(2,1)S(1)} fusion(bf16[3,2048,1024]{2,1,0:T(8,128)(2,1)} %all-gather.7.cloned.1.call-done, bf16[640,2048]{1,0:T(8,128)(2,1)} %all-gather.9.cloned.1.call-done), kind=kOutput, calls=%fused_computation.1 | convolution fusion | flops 8055029760 | bytes 19136512 | tf_op jit(solution)/shard_map/td,kdc->ktc/dot_general | solution.py:29
  216.9 1.9 copy-done.2
  218.7 0.5 multiply_bitcast_fusion
  219.2 60.5 %all-gather.11.cloned.1.call-done = bf16[1024,2048]{1,0:T(8,128)(2,1)} async-done(((bf16[1024,256]{1,0:T(8,128)(2,1)}), bf16[1024,2048]{1,0:T(8,128)(2,1)}) %all-gather.11.cloned.1.call-update) | async-done | bytes 4194320 | tf_op jit(solution)/shard_map/all_gather | solution.py:38
  279.7 7.4 %convolution_convert_fusion.1 = bf16[640,2048]{1,0:T(8,128)(2,1)} fusion(bf16[1024,2048]{1,0:T(8,128)(2,1)} %all-gather.11.cloned.1.call-done, f32[640,1024]{1,0:T(8,128)S(1)} %multiply_bitcast_fusion, bf16[3,640,1024]{2,1,0:T(8,128)(2,1)} %copy-done.2, f32[1024]{0:T(1024)S(1)} %bitcast.51, f32[1024]{0:T(1024)S(1)} %bitcast.50, f32[1024]{0:T(1024)S(1)} %bitcast.49), kind=kOutput, calls=%fused_computation.10 | convolution fusion | flops 2690908160 | bytes 10760192 | tf_op jit(solution)/shard_map/dot_general | solution.py:43
  287.1 0.0 all-gather.13.cloned.1.call-start
  287.2 1.0 copy-done.3
  288.2 0.3 copy.12
  288.5 0.3 copy.13
  288.8 1.3 pad_maximum_fusion.1
  290.1 0.0 all-gather.15.cloned.1.call-start
  290.2 5.7 reduce-scatter.3.cloned.1.call-done
  295.9 1.9 multiply_reduce_fusion
  297.9 1.6 multiply_convert_fusion
  299.6 0.7 all-gather.17.cloned.1.call-update
  300.3 0.2 reduce-scatter.5.cloned.1.call-start
  300.5 161.9 %all-gather.13.cloned.1.call-done = bf16[2,2048,1408]{1,2,0:T(8,128)(2,1)} async-done(((bf16[2,256,1408]{1,2,0:T(8,128)(2,1)}), bf16[2,2048,1408]{1,2,0:T(8,128)(2,1)}) %all-gather.13.cloned.1.call-update) | async-done | bytes 11534352 | tf_op jit(solution)/shard_map/all_gather | solution.py:32
  462.4 11.0 %all-gather.15.cloned.1.call-done = bf16[640,2048]{1,0:T(8,128)(2,1)} async-done(((bf16[320,2048]{1,0:T(8,128)(2,1)}), bf16[640,2048]{1,0:T(8,128)(2,1)}) %all-gather.15.cloned.1.call-update) | async-done | bytes 2621456 | tf_op jit(solution)/shard_map/all_gather | solution.py:25
  473.4 14.6 %convolution_bitcast_fusion = f32[2,640,1408]{1,2,0:T(8,128)} fusion(bf16[2,2048,1408]{1,2,0:T(8,128)(2,1)} %all-gather.13.cloned.1.call-done, bf16[640,2048]{1,0:T(8,128)(2,1)} %all-gather.15.cloned.1.call-done), kind=kOutput, calls=%fused_computation | convolution fusion | flops 7381975040 | bytes 21364736 | tf_op jit(solution)/shard_map/td,kdc->ktc/dot_general | solution.py:29
  488.0 81.8 %all-gather.17.cloned.1.call-done = bf16[1408,2048]{1,0:T(8,128)(2,1)} async-done(((bf16[1408,256]{1,0:T(8,128)(2,1)}), bf16[1408,2048]{1,0:T(8,128)(2,1)}) %all-gather.17.cloned.1.call-update) | async-done | bytes 5767184 | tf_op jit(solution)/shard_map/all_gather | solution.py:38
  569.8 10.7 %convolution_convert_fusion = bf16[640,2048]{1,0:T(8,128)(2,1)} fusion(bf16[1408,2048]{1,0:T(8,128)(2,1)} %all-gather.17.cloned.1.call-done, f32[2,640,1408]{1,2,0:T(8,128)} %convolution_bitcast_fusion), kind=kOutput, calls=%fused_computation.9 | convolution fusion | flops 3697704960 | bytes 15597568 | tf_op jit(solution)/shard_map/dot_general | solution.py:43
  580.5 8.8 %reduce-scatter.5.cloned.1.call-done = bf16[320,2048]{1,0:T(8,128)(2,1)} async-done(((bf16[640,2048]{1,0:T(8,128)(2,1)}), bf16[320,2048]{1,0:T(8,128)(2,1)}) %reduce-scatter.5.cloned.1.call-update) | async-done | bytes 1310736 | tf_op jit(solution)/shard_map/reduce_scatter | solution.py:42
  589.3 3.1 add_convert_fusion
  (27 shorter events, 0.2 us)
Async XLA Ops:
  6.5 18.8 %all-gather.9.cloned.1.call-start = ((), (), s32[]{:S(2)}) async-start(), calls=%async_computation.3 | async-start | bytes 3932160 | tf_op jit(solution)/shard_map/all_gather | solution.py:25
  6.5 4.6 copy-start.5
  6.5 4.6 copy-start.6
  6.5 4.6 copy-start.7
  11.1 193.7 %all-gather.7.cloned.1.call-start = ((), (), s32[]{:S(2)}) async-start(), calls=%async_computation.2 | async-start | bytes 14155776 | tf_op jit(solution)/shard_map/all_gather | solution.py:32
  12.5 267.2 %all-gather.11.cloned.1.call-start = ((), (), s32[]{:S(2)}) async-start(), calls=%async_computation.4 | async-start | bytes 4718592 | tf_op jit(solution)/shard_map/all_gather | solution.py:38
  13.3 282.6 %reduce-scatter.3.cloned.1.call-start = ((), (), s32[]{:S(2)}) async-start(), calls=%async_computation.5 | async-start | bytes 3932160 | tf_op jit(solution)/shard_map/reduce_scatter | solution.py:42
  216.9 1.9 copy-start.2
  287.1 1.1 copy-start.3
  287.1 1.4 copy-start.4
  287.1 175.3 %all-gather.13.cloned.1.call-start = ((), (), s32[]{:S(2)}) async-start(), calls=%async_computation.6 | async-start | bytes 12976128 | tf_op jit(solution)/shard_map/all_gather | solution.py:32
  288.5 7.4 %copy-start = (bf16[320,2048]{1,0:T(8,128)(2,1)S(1)}, bf16[320,2048]{1,0:T(8,128)(2,1)}, u32[]{:S(2)}) copy-start(bf16[320,2048]{1,0:T(8,128)(2,1)} %param.11) | copy-start | bytes 3932164
  290.1 7.8 %copy-start.8 = (f32[2048]{0:T(1024)S(1)}, f32[2048]{0:T(1024)}, u32[]{:S(2)}) copy-start(f32[2048]{0:T(1024)} %param.18) | copy-start | bytes 24580
  290.1 183.3 %all-gather.15.cloned.1.call-start = ((), (), s32[]{:S(2)}) async-start(), calls=%async_computation.7 | async-start | bytes 3932160 | tf_op jit(solution)/shard_map/all_gather | solution.py:25
  295.9 2.0 copy-start.1
  299.5 270.3 %all-gather.17.cloned.1.call-start = ((), (), s32[]{:S(2)}) async-start(), calls=%async_computation.8 | async-start | bytes 6488064 | tf_op jit(solution)/shard_map/all_gather | solution.py:38
  300.3 289.0 %reduce-scatter.5.cloned.1.call-start = ((), (), s32[]{:S(2)}) async-start(), calls=%async_computation.9 | async-start | bytes 3932160 | tf_op jit(solution)/shard_map/reduce_scatter | solution.py:42
Sparse Core Ops, SparseCore 0:
  11.2 14.0 all-gather.8
  27.5 177.2 all-gather.6
  206.9 72.7 all-gather.10
  287.2 8.6 reduce-scatter.2
  297.8 164.5 all-gather.12
  463.8 9.5 all-gather.14
  475.4 94.3 all-gather.16
  580.6 8.6 reduce-scatter.4
where the time goes:
time: 599 us
  waiting for transfers between devices  522 us (87%)
  matrix products  44.7 us (7%)
  other arithmetic  14.3 us (2%)
  between operations  13.6 us (2%)
    all_gather x2, waiting for transfers between devices, project_in(): lax.all_gather(stacked, 'fs', axis=1, tiled=True)  341 us
    all_gather x2, waiting for transfers between devices, collect_out(): return lax.all_gather(weight, 'fs', axis=1, tiled=True)  142 us
    dot_general x2, matrix products, project_in(): jnp.einsum('td,kdc->ktc', gathered, lax.all_gather(stacked, 'fs', axis=1,...  26.7 us
    all_gather x2, waiting for transfers between devices, gather_rows(): return lax.all_gather(normed, 'tp', axis=0, tiled=True)  22 us
    dot_general x2, matrix products, sum_parts(): jnp.dot(local_cols, weight, preferred_element_type=jnp.float32)  18 us
    reduce_scatter x2, waiting for transfers between devices, sum_parts(): lax.psum_scatter(jnp.dot(local_cols, weight, preferred_element_type=jnp.f...  14.5 us
  transfers between devices with their start and end apart: 8, of which 8 were waited for; matrix products, arithmetic and copies ran while one was open for 6% of the time, Pallas kernels for 0%

commit v1 on v0

--- a/solution.py
+++ b/solution.py
@@ -2,6 +2,18 @@
 import jax.numpy as jnp
 from jax import lax
 from jax.sharding import PartitionSpec as P
+
+
+def ring_product(x, axis, dim, contribution):
+    length, index = (lax.axis_size(axis), lax.axis_index(axis))
+    behind = [(i, (i - 1) % length) for i in range(length)]
+    width = x.shape[dim]
+    current = x
+    so_far = contribution(current, index * width)
+    for step in range(1, length):
+        current = lax.ppermute(current, axis, behind)
+        so_far = so_far + contribution(current, (index + step) % length * width)
+    return so_far
 
 
 def rms_scale(matrix, gain):
@@ -26,11 +38,16 @@
 
 
 def project_in(gathered, stacked):
-    return jnp.einsum(
-        "td,kdc->ktc",
-        gathered,
-        lax.all_gather(stacked, "fs", axis=1, tiled=True),
-        preferred_element_type=jnp.float32,
+    return ring_product(
+        stacked,
+        "fs",
+        1,
+        lambda own_block, at: jnp.einsum(
+            "td,kdc->ktc",
+            lax.dynamic_slice_in_dim(gathered, at, own_block.shape[1], axis=1),
+            own_block,
+            preferred_element_type=jnp.float32,
+        ),
     )
 
 

time: 599 us -> 709 us (1.18)
  matrix products: 44.7 us -> 133 us
  starting transfers between devices: 0.47 us -> 73.6 us
  waiting for transfers between devices: 522 us -> 467 us
    ppermute x0 -> x14, waiting for transfers between devices: none -> 455 us  [ring_product(): current = lax.ppermute(current, axis, behind)]
    all_gather x2 -> x0, waiting for transfers between devices: 341 us -> none  [project_in(): lax.all_gather(stacked, 'fs', axis=1, tiled=True)]
    all_gather x2, waiting for transfers between devices: 142 us -> 0.01 us  [collect_out(): return lax.all_gather(weight, 'fs', axis=1, tiled=True)]
    dot_general x2 -> x16, matrix products: 26.7 us -> 112 us  [project_in(): jnp.einsum('td,kdc->ktc', lax.dynamic_slice_in_dim(gathered, at, own_bloc...]
    ppermute x0 -> x14, starting transfers between devices: none -> 73.4 us  [ring_product(): current = lax.ppermute(current, axis, behind)]
    all_gather x2, waiting for transfers between devices: 22 us -> 0.02 us  [gather_rows(): return lax.all_gather(normed, 'tp', axis=0, tiled=True)]
  transfers between devices with their start and end apart: 8 -> 20, of which waited for: 8 -> 15; matrix products, arithmetic and copies ran while one was open for 6% -> 18% of each run, Pallas kernels for 0% -> 0%
where the time goes in v1:
time: 709 us; the launch traced here: 708 us
  waiting for transfers between devices  467 us (66%)
  matrix products  133 us (19%)
  starting transfers between devices  73.6 us (10%)
  other arithmetic  15.1 us (2%)
  between operations  13.6 us (2%)
    ppermute x14, waiting for transfers between devices, ring_product(): current = lax.ppermute(current, axis, behind)  455 us
    dot_general x16, matrix products, project_in(): jnp.einsum('td,kdc->ktc', lax.dynamic_slice_in_dim(gathered, at, own_bloc...  112 us
    ppermute x14, starting transfers between devices, ring_product(): current = lax.ppermute(current, axis, behind)  73.4 us
    dot_general x2, matrix products, sum_parts(): jnp.dot(local_cols, weight, preferred_element_type=jnp.float32)  20.8 us
  transfers between devices with their start and end apart: 20, of which 15 were waited for; matrix products, arithmetic and copies ran while one was open for 18% of the time, Pallas kernels for 0%

profile of v1, /device:TPU:0, one launch (start us, length us, event | category | flops | bytes accessed | tf_op | source)
XLA Modules:
  0.0 708.0 jit_solution(13793187216928239497)
XLA Ops:
  8.2 6.1 collective-permute-start
  14.3 33.7 %collective-permute-done = bf16[3,256,1024]{2,1,0:T(8,128)(2,1)S(1)} collective-permute-done((bf16[3,256,1024]{2,1,0:T(8,128)(2,1)S(1)}, bf16[3,256,1024]{2,1,0:T(8,128)(2,1)S(1)}, u32[]{:S(2)}, u32[]{:S(2)}) %collective-permute-start) | collective-permute-done | bytes 1572896 | tf_op jit(solution)/shard_map/ppermute | solution.py:14
  53.1 32.8 %collective-permute-done.1 = bf16[3,256,1024]{2,1,0:T(8,128)(2,1)} collective-permute-done((bf16[3,256,1024]{2,1,0:T(8,128)(2,1)S(1)}, bf16[3,256,1024]{2,1,0:T(8,128)(2,1)}, u32[]{:S(2)}, u32[]{:S(2)}) %collective-permute-start.1) | collective-permute-done | bytes 1572896 | tf_op jit(solution)/shard_map/ppermute | solution.py:14
  85.9 5.3 collective-permute-start.2
  93.1 30.4 %collective-permute-done.2 = bf16[3,256,1024]{2,1,0:T(8,128)(2,1)} collective-permute-done((bf16[3,256,1024]{2,1,0:T(8,128)(2,1)}, bf16[3,256,1024]{2,1,0:T(8,128)(2,1)}, u32[]{:S(2)}, u32[]{:S(2)}) %collective-permute-start.2) | collective-permute-done | bytes 1572896 | tf_op jit(solution)/shard_map/ppermute | solution.py:14
  128.6 31.4 %collective-permute-done.3 = bf16[3,256,1024]{2,1,0:T(8,128)(2,1)} collective-permute-done((bf16[3,256,1024]{2,1,0:T(8,128)(2,1)}, bf16[3,256,1024]{2,1,0:T(8,128)(2,1)}, u32[]{:S(2)}, u32[]{:S(2)}) %collective-permute-start.3) | collective-permute-done | bytes 1572896 | tf_op jit(solution)/shard_map/ppermute | solution.py:14
  165.3 47.4 %collective-permute-done.4 = bf16[3,256,1024]{2,1,0:T(8,128)(2,1)} collective-permute-done((bf16[3,256,1024]{2,1,0:T(8,128)(2,1)}, bf16[3,256,1024]{2,1,0:T(8,128)(2,1)}, u32[]{:S(2)}, u32[]{:S(2)}) %collective-permute-start.4) | collective-permute-done | bytes 1572896 | tf_op jit(solution)/shard_map/ppermute | solution.py:14
  218.8 5.8 fusion.41
  225.8 5.7 fusion.37
  231.5 51.9 %collective-permute-done.5 = bf16[3,256,1024]{2,1,0:T(8,128)(2,1)} collective-permute-done((bf16[3,256,1024]{2,1,0:T(8,128)(2,1)}, bf16[3,256,1024]{2,1,0:T(8,128)(2,1)}, u32[]{:S(2)}, u32[]{:S(2)}) %collective-permute-start.5) | collective-permute-done | bytes 1572896 | tf_op jit(solution)/shard_map/ppermute | solution.py:14
  288.5 5.7 fusion.35
  294.2 5.8 fusion.33
  300.0 5.7 fusion.31
  305.7 5.8 fusion.29
  314.8 17.7 %fusion = bf16[3,640,1024]{2,1,0:T(8,128)(2,1)} fusion(f32[3,1024,640]{1,2,0:T(8,128)} %fusion.29, f32[3,1024,640]{1,2,0:T(8,128)} %fusion.31, f32[3,1024,640]{1,2,0:T(8,128)} %fusion.33, f32[3,1024,640]{1,2,0:T(8,128)} %fusion.35, f32[3,1024,640]{1,2,0:T(8,128)} %fusion.37, f32[3,1024,640]{1,2,0:T(8,128)} %fusion.41, f32[3,1024,640]{1,2,0:T(8,128)S(1)} %fusion.39, ...), kind=kOutput, calls=%fused_computation.2 | convolution fusion | flops 1022361600 | bytes 60882948 | tf_op jit(solution)/shard_map/td,kdc->ktc/dot_general | solution.py:45
  336.3 9.9 %convolution_convert_fusion.1 = bf16[640,2048]{1,0:T(8,128)(2,1)} fusion(bf16[1024,2048]{1,0:T(8,128)(2,1)} %all-gather.7.cloned.1.call-done, f32[640,1024]{1,0:T(8,128)} %multiply_bitcast_fusion, bf16[3,640,1024]{2,1,0:T(8,128)(2,1)} %fusion, f32[1024]{0:T(1024)S(1)} %bitcast.108, f32[1024]{0:T(1024)S(1)} %bitcast.107, f32[1024]{0:T(1024)S(1)} %bitcast.106), kind=kOutput, calls=%fused_computation.11 | convolution fusion | flops 2690908160 | bytes 10760192 | tf_op jit(solution)/shard_map/dot_general | solution.py:60
  362.3 19.6 %collective-permute-done.7 = bf16[2,256,1408]{1,2,0:T(8,128)(2,1)} collective-permute-done((bf16[2,256,1408]{1,2,0:T(8,128)(2,1)}, bf16[2,256,1408]{1,2,0:T(8,128)(2,1)}, u32[]{:S(2)}, u32[]{:S(2)}) %collective-permute-start.7) | collective-permute-done | bytes 1441824 | tf_op jit(solution)/shard_map/ppermute | solution.py:14
  387.1 26.6 %collective-permute-done.8 = bf16[2,256,1408]{1,2,0:T(8,128)(2,1)} collective-permute-done((bf16[2,256,1408]{1,2,0:T(8,128)(2,1)}, bf16[2,256,1408]{1,2,0:T(8,128)(2,1)}, u32[]{:S(2)}, u32[]{:S(2)}) %collective-permute-start.8) | collective-permute-done | bytes 1441824 | tf_op jit(solution)/shard_map/ppermute | solution.py:14
  418.9 53.2 %collective-permute-done.9 = bf16[2,256,1408]{1,2,0:T(8,128)(2,1)} collective-permute-done((bf16[2,256,1408]{1,2,0:T(8,128)(2,1)}, bf16[2,256,1408]{1,2,0:T(8,128)(2,1)}, u32[]{:S(2)}, u32[]{:S(2)}) %collective-permute-start.9) | collective-permute-done | bytes 1441824 | tf_op jit(solution)/shard_map/ppermute | solution.py:14
  477.3 26.3 %collective-permute-done.10 = bf16[2,256,1408]{1,2,0:T(8,128)(2,1)S(1)} collective-permute-done((bf16[2,256,1408]{1,2,0:T(8,128)(2,1)}, bf16[2,256,1408]{1,2,0:T(8,128)(2,1)S(1)}, u32[]{:S(2)}, u32[]{:S(2)}) %collective-permute-start.10) | collective-permute-done | bytes 1441824 | tf_op jit(solution)/shard_map/ppermute | solution.py:14
  509.8 48.2 %collective-permute-done.11 = bf16[2,256,1408]{1,2,0:T(8,128)(2,1)S(1)} collective-permute-done((bf16[2,256,1408]{1,2,0:T(8,128)(2,1)S(1)}, bf16[2,256,1408]{1,2,0:T(8,128)(2,1)S(1)}, u32[]{:S(2)}, u32[]{:S(2)}) %collective-permute-start.11) | collective-permute-done | bytes 1441824 | tf_op jit(solution)/shard_map/ppermute | solution.py:14
  559.1 5.2 collective-permute-start.12
  564.3 50.5 %collective-permute-done.12 = bf16[2,256,1408]{1,2,0:T(8,128)(2,1)} collective-permute-done((bf16[2,256,1408]{1,2,0:T(8,128)(2,1)S(1)}, bf16[2,256,1408]{1,2,0:T(8,128)(2,1)}, u32[]{:S(2)}, u32[]{:S(2)}) %collective-permute-start.12) | collective-permute-done | bytes 1441824 | tf_op jit(solution)/shard_map/ppermute | solution.py:14
  614.8 5.3 collective-permute-start.13
  620.1 5.8 fusion.18
  625.9 5.8 fusion.20
  640.2 5.6 fusion.22
  645.8 5.7 fusion.24
  651.5 5.6 fusion.14
  657.1 21.8 %add_bitcast_fusion = f32[2,640,1408]{1,2,0:T(8,128)} fusion(f32[2,1408,640]{2,1,0:T(8,128)} %fusion.14, f32[2,1408,640]{2,1,0:T(8,128)} %fusion.16, f32[2,1408,640]{2,1,0:T(8,128)} %fusion.18, f32[2,1408,640]{2,1,0:T(8,128)} %fusion.20, f32[2,1408,640]{2,1,0:T(8,128)} %fusion.22, f32[2,1408,640]{2,1,0:T(8,128)} %fusion.26, f32[2,1408,640]{2,1,0:T(8,128)} %fusion.24, ...), kind=kOutput, calls=%fused_computation.1 | convolution fusion | flops 935362560 | bytes 59441156 | tf_op jit(solution)/shard_map/td,kdc->ktc/dot_general | solution.py:45
  678.9 10.9 %convolution_convert_fusion = bf16[640,2048]{1,0:T(8,128)(2,1)} fusion(bf16[1408,2048]{1,0:T(8,128)(2,1)} %all-gather.11.cloned.1.call-done, f32[2,640,1408]{1,2,0:T(8,128)} %add_bitcast_fusion), kind=kOutput, calls=%fused_computation.10 | convolution fusion | flops 3697704960 | bytes 15597568 | tf_op jit(solution)/shard_map/dot_general | solution.py:60
  689.8 8.2 %reduce-scatter.5.cloned.1.call-done = bf16[320,2048]{1,0:T(8,128)(2,1)} async-done(((bf16[640,2048]{1,0:T(8,128)(2,1)}), bf16[320,2048]{1,0:T(8,128)(2,1)}) %reduce-scatter.5.cloned.1.call-update) | async-done | bytes 1310736 | tf_op jit(solution)/shard_map/reduce_scatter | solution.py:59
  (71 shorter events, 89.2 us)
Async XLA Ops:
  6.5 84.6 %copy-start = (bf16[320,2048]{1,0:T(8,128)(2,1)S(1)}, bf16[320,2048]{1,0:T(8,128)(2,1)}, u32[]{:S(2)}) copy-start(bf16[320,2048]{1,0:T(8,128)(2,1)} %param.11) | copy-start | bytes 3932164
  6.5 85.0 %copy-start.11 = (f32[2048]{0:T(1024)S(1)}, f32[2048]{0:T(1024)}, u32[]{:S(2)}) copy-start(f32[2048]{0:T(1024)} %param.12) | copy-start | bytes 24580
  6.5 212.2 %all-gather.5.cloned.1.call-start = ((), (), s32[]{:S(2)}) async-start(), calls=%async_computation.2 | async-start | bytes 3932160 | tf_op jit(solution)/shard_map/all_gather | solution.py:37
  8.2 39.7 %collective-permute-start = (bf16[3,256,1024]{2,1,0:T(8,128)(2,1)S(1)}, bf16[3,256,1024]{2,1,0:T(8,128)(2,1)S(1)}, u32[]{:S(2)}, u32[]{:S(2)}) collective-permute-start(bf16[3,256,1024]{2,1,0:T(8,128)(2,1)S(1)} %pad_maximum_fusion), channel_id=1, source_target_pairs={{0,14},{2,0},{4,2},{6,4},{8,6},{10,8},{12,10},{14,12},{1,15},{3,1}... | collective-permute-start | bytes 4718600 | tf_op jit(solution)/shard_map/ppermute | solution.py:14
  47.9 38.0 %collective-permute-start.1 = (bf16[3,256,1024]{2,1,0:T(8,128)(2,1)S(1)}, bf16[3,256,1024]{2,1,0:T(8,128)(2,1)}, u32[]{:S(2)}, u32[]{:S(2)}) collective-permute-start(bf16[3,256,1024]{2,1,0:T(8,128)(2,1)S(1)} %collective-permute-done), channel_id=1, source_target_pairs={{0,14},{2,0},{4,2},{6,4},{8,6},{10,8},{12,10},{14,12},{1,15},{3,1}... | collective-permute-start | bytes 4718600 | tf_op jit(solution)/shard_map/ppermute | solution.py:14
  85.9 37.5 %collective-permute-start.2 = (bf16[3,256,1024]{2,1,0:T(8,128)(2,1)}, bf16[3,256,1024]{2,1,0:T(8,128)(2,1)}, u32[]{:S(2)}, u32[]{:S(2)}) collective-permute-start(bf16[3,256,1024]{2,1,0:T(8,128)(2,1)} %collective-permute-done.1), channel_id=1, source_target_pairs={{0,14},{2,0},{4,2},{6,4},{8,6},{10,8},{12,10},{14,12},{1,15},{3,1}... | collective-permute-start | bytes 4718600 | tf_op jit(solution)/shard_map/ppermute | solution.py:14
  91.5 127.2 %copy-start.6 = (bf16[256,1024]{1,0:T(8,128)(2,1)S(1)}, bf16[256,1024]{1,0:T(8,128)(2,1)}, u32[]{:S(2)}) copy-start(bf16[256,1024]{1,0:T(8,128)(2,1)} %param.15) | copy-start | bytes 1572868
  93.0 243.3 %all-gather.7.cloned.1.call-start = ((), (), s32[]{:S(2)}) async-start(), calls=%async_computation.3 | async-start | bytes 4718592 | tf_op jit(solution)/shard_map/all_gather | solution.py:55
  123.4 36.6 %collective-permute-start.3 = (bf16[3,256,1024]{2,1,0:T(8,128)(2,1)}, bf16[3,256,1024]{2,1,0:T(8,128)(2,1)}, u32[]{:S(2)}, u32[]{:S(2)}) collective-permute-start(bf16[3,256,1024]{2,1,0:T(8,128)(2,1)} %collective-permute-done.2), channel_id=1, source_target_pairs={{0,14},{2,0},{4,2},{6,4},{8,6},{10,8},{12,10},{14,12},{1,15},{3,1}... | collective-permute-start | bytes 4718600 | tf_op jit(solution)/shard_map/ppermute | solution.py:14
  160.0 52.6 %collective-permute-start.4 = (bf16[3,256,1024]{2,1,0:T(8,128)(2,1)}, bf16[3,256,1024]{2,1,0:T(8,128)(2,1)}, u32[]{:S(2)}, u32[]{:S(2)}) collective-permute-start(bf16[3,256,1024]{2,1,0:T(8,128)(2,1)} %collective-permute-done.3), channel_id=1, source_target_pairs={{0,14},{2,0},{4,2},{6,4},{8,6},{10,8},{12,10},{14,12},{1,15},{3,1}... | collective-permute-start | bytes 4718600 | tf_op jit(solution)/shard_map/ppermute | solution.py:14
  165.2 193.4 %reduce-scatter.3.cloned.1.call-start = ((), (), s32[]{:S(2)}) async-start(), calls=%async_computation.4 | async-start | bytes 3932160 | tf_op jit(solution)/shard_map/reduce_scatter | solution.py:59
  212.6 70.7 %collective-permute-start.5 = (bf16[3,256,1024]{2,1,0:T(8,128)(2,1)}, bf16[3,256,1024]{2,1,0:T(8,128)(2,1)}, u32[]{:S(2)}, u32[]{:S(2)}) collective-permute-start(bf16[3,256,1024]{2,1,0:T(8,128)(2,1)} %collective-permute-done.4), channel_id=1, source_target_pairs={{0,14},{2,0},{4,2},{6,4},{8,6},{10,8},{12,10},{14,12},{1,15},{3,1}... | collective-permute-start | bytes 4718600 | tf_op jit(solution)/shard_map/ppermute | solution.py:14
  218.8 5.8 copy-start.4
  283.3 31.5 %collective-permute-start.6 = (bf16[3,256,1024]{2,1,0:T(8,128)(2,1)}, bf16[3,256,1024]{2,1,0:T(8,128)(2,1)S(1)}, u32[]{:S(2)}, u32[]{:S(2)}) collective-permute-start(bf16[3,256,1024]{2,1,0:T(8,128)(2,1)} %collective-permute-done.5), channel_id=1, source_target_pairs={{0,14},{2,0},{4,2},{6,4},{8,6},{10,8},{12,10},{14,12},{1,15},{3,1}... | collective-permute-start | bytes 4718600 | tf_op jit(solution)/shard_map/ppermute | solution.py:14
  346.1 1.1 copy-start.10
  346.2 273.9 %all-gather.9.cloned.1.call-start = ((), (), s32[]{:S(2)}) async-start(), calls=%async_computation.5 | async-start | bytes 3932160 | tf_op jit(solution)/shard_map/all_gather | solution.py:37
  348.9 6.4 copy-start.2
  348.9 11.6 %copy-start.12 = (f32[2048]{0:T(1024)S(1)}, f32[2048]{0:T(1024)}, u32[]{:S(2)}) copy-start(f32[2048]{0:T(1024)} %param.18) | copy-start | bytes 24580
  350.3 31.6 %collective-permute-start.7 = (bf16[2,256,1408]{1,2,0:T(8,128)(2,1)}, bf16[2,256,1408]{1,2,0:T(8,128)(2,1)}, u32[]{:S(2)}, u32[]{:S(2)}) collective-permute-start(bf16[2,256,1408]{1,2,0:T(8,128)(2,1)} %pad_maximum_fusion.1), channel_id=1, source_target_pairs={{0,14},{2,0},{4,2},{6,4},{8,6},{10,8},{12,10},{14,12},{1,15},{3,1}... | collective-permute-start | bytes 4325384 | tf_op jit(solution)/shard_map/ppermute | solution.py:14
  358.6 2.0 copy-start.1
  362.2 316.6 %all-gather.11.cloned.1.call-start = ((), (), s32[]{:S(2)}) async-start(), calls=%async_computation.6 | async-start | bytes 6488064 | tf_op jit(solution)/shard_map/all_gather | solution.py:55
  381.9 31.7 %collective-permute-start.8 = (bf16[2,256,1408]{1,2,0:T(8,128)(2,1)}, bf16[2,256,1408]{1,2,0:T(8,128)(2,1)}, u32[]{:S(2)}, u32[]{:S(2)}) collective-permute-start(bf16[2,256,1408]{1,2,0:T(8,128)(2,1)} %collective-permute-done.7), channel_id=1, source_target_pairs={{0,14},{2,0},{4,2},{6,4},{8,6},{10,8},{12,10},{14,12},{1,15},{3,1}... | collective-permute-start | bytes 4325384 | tf_op jit(solution)/shard_map/ppermute | solution.py:14
  413.7 58.4 %collective-permute-start.9 = (bf16[2,256,1408]{1,2,0:T(8,128)(2,1)}, bf16[2,256,1408]{1,2,0:T(8,128)(2,1)}, u32[]{:S(2)}, u32[]{:S(2)}) collective-permute-start(bf16[2,256,1408]{1,2,0:T(8,128)(2,1)} %collective-permute-done.8), channel_id=1, source_target_pairs={{0,14},{2,0},{4,2},{6,4},{8,6},{10,8},{12,10},{14,12},{1,15},{3,1}... | collective-permute-start | bytes 4325384 | tf_op jit(solution)/shard_map/ppermute | solution.py:14
  418.9 279.2 %reduce-scatter.5.cloned.1.call-start = ((), (), s32[]{:S(2)}) async-start(), calls=%async_computation.7 | async-start | bytes 3932160 | tf_op jit(solution)/shard_map/reduce_scatter | solution.py:59
  472.1 31.4 %collective-permute-start.10 = (bf16[2,256,1408]{1,2,0:T(8,128)(2,1)}, bf16[2,256,1408]{1,2,0:T(8,128)(2,1)S(1)}, u32[]{:S(2)}, u32[]{:S(2)}) collective-permute-start(bf16[2,256,1408]{1,2,0:T(8,128)(2,1)} %collective-permute-done.9), channel_id=1, source_target_pairs={{0,14},{2,0},{4,2},{6,4},{8,6},{10,8},{12,10},{14,12},{1,15},{3,1}... | collective-permute-start | bytes 4325384 | tf_op jit(solution)/shard_map/ppermute | solution.py:14
  503.5 1.2 copy-start.7
  504.7 53.3 %collective-permute-start.11 = (bf16[2,256,1408]{1,2,0:T(8,128)(2,1)S(1)}, bf16[2,256,1408]{1,2,0:T(8,128)(2,1)S(1)}, u32[]{:S(2)}, u32[]{:S(2)}) collective-permute-start(bf16[2,256,1408]{1,2,0:T(8,128)(2,1)S(1)} %collective-permute-done.10), channel_id=1, source_target_pairs={{0,14},{2,0},{4,2},{6,4},{8,6},{10,8},{12,10},{14,12},{1,15},{3,1}... | collective-permute-start | bytes 4325384 | tf_op jit(solution)/shard_map/ppermute | solution.py:14
  559.1 55.7 %collective-permute-start.12 = (bf16[2,256,1408]{1,2,0:T(8,128)(2,1)S(1)}, bf16[2,256,1408]{1,2,0:T(8,128)(2,1)}, u32[]{:S(2)}, u32[]{:S(2)}) collective-permute-start(bf16[2,256,1408]{1,2,0:T(8,128)(2,1)S(1)} %collective-permute-done.11), channel_id=1, source_target_pairs={{0,14},{2,0},{4,2},{6,4},{8,6},{10,8},{12,10},{14,12},{1,15},{3,1}... | collective-permute-start | bytes 4325384 | tf_op jit(solution)/shard_map/ppermute | solution.py:14
  614.8 42.2 %collective-permute-start.13 = (bf16[2,256,1408]{1,2,0:T(8,128)(2,1)}, bf16[2,256,1408]{1,2,0:T(8,128)(2,1)}, u32[]{:S(2)}, u32[]{:S(2)}) collective-permute-start(bf16[2,256,1408]{1,2,0:T(8,128)(2,1)} %collective-permute-done.12), channel_id=1, source_target_pairs={{0,14},{2,0},{4,2},{6,4},{8,6},{10,8},{12,10},{14,12},{1,15},{3,1}... | collective-permute-start | bytes 4325384 | tf_op jit(solution)/shard_map/ppermute | solution.py:14
  620.1 5.8 copy-start.5
  625.9 5.8 copy-start.9
  631.7 4.2 copy-start.3
  (1 other events, 1.1 us)
Sparse Core Ops, SparseCore 0:
  93.1 8.5 all-gather.4
  165.3 119.3 all-gather.6
  346.3 12.2 reduce-scatter.2
  362.4 12.6 all-gather.8
  419.0 185.4 all-gather.10
  690.0 8.0 reduce-scatter.4
